TPU v7x, 512 devices: a 8x2x16 block of a 8x8x16 slice. The times are simulated.
512 devices in a mesh: grp: 2 (over y), sp: 32 (over z, core), tp: 8 (over x).
Axes of the slice: x: 8, y: 2, z: 16, core: 2. Of those that a mesh axis runs over, the one named last changes fastest.
The devices are a block of a 8x8x16 slice.
Arguments:
- residual: bfloat16 [16384, 2048], P(('grp', 'sp')), parts along dimension 0, may hold values from -34 to 34
- queries: bfloat16 [16384, 1024], P(('grp', 'sp'), 'tp'), parts along dimension 0, may hold values from -400 to 400
- keys: bfloat16 [16384, 512], P(('grp', 'sp'), 'tp'), parts along dimension 0, may hold values from -8 to 8
- values: bfloat16 [16384, 512], P(('grp', 'sp'), 'tp'), parts along dimension 0, may hold values from -6 to 6
- segments: int32 [16384], P(('grp', 'sp')), parts along dimension 0, may hold values from 0 to 16, never falling along the last dimension, each value on 1 to 768 neighbouring positions
- routes: int32 [16384, 2], P(('grp', 'sp')), parts along dimension 0, may hold values from 0 to 31, all different within a row; in each aligned block of 256 rows (0 to 255, 256 to 511, ...) at most 32 rows name the same one
- route_weight: float32 [16384, 2], P(('grp', 'sp')), parts along dimension 0, may hold values from 0.3 to 3
- sinks: float32 [16], P('tp'), may hold values from 1 to 6
- out_weight: bfloat16 [1024, 2048], P('tp'), may hold values from -1 to 1
- norm_gain: float32 [2048], replicated, may hold values from 0.1 to 1.9
- expert_gate: bfloat16 [32, 2048, 1024], P('sp', None, 'tp'), may hold values from -0.125 to 0.125
- expert_up: bfloat16 [32, 2048, 1024], P('sp', None, 'tp'), may hold values from -0.125 to 0.125
- expert_down: bfloat16 [32, 1024, 2048], P('sp', None, 'tp'), may hold values from -0.1875 to 0.1875
- shared_gate: bfloat16 [2048, 1024], P(None, 'tp'), may hold values from -0.125 to 0.125
- shared_up: bfloat16 [2048, 1024], P(None, 'tp'), may hold values from -0.125 to 0.125
- shared_down: bfloat16 [1024, 2048], P(None, 'tp'), may hold values from -0.1875 to 0.1875
Outputs:
- mixed: bfloat16 [16384, 2048], P(('grp', 'sp'), 'tp'), parts along dimension 0
There are 2 independent parts, one for each index of `grp`. A program takes and returns all parts, laid end to end along the dimension named above; an argument that names none is the same for every part. Nothing has to cross between parts.
Inputs may be any that keep to these rules, and one draw needn't show every extreme that they name: `routes`: each row names 2 different experts. In the rows of one device no expert is named by more than 32 rows, and in some device's rows an expert is named by exactly 32. `segments`: document numbers never fall along the positions; every document spans 1 to 768 positions and one spans exactly 768.
All inputs are finite; a program needn't handle non-finite values.
Results may differ from a plain program's by a relative error of at most 0.0065.
Values may be sent and summed in bfloat16 or wider, within the bound.
A program may use at most 64 MiB of HBM per device.

v0:
```python
import jax
import jax.numpy as jnp
from jax import lax
from jax.sharding import Mesh
from jax.sharding import PartitionSpec as P

HEAD_DIM = 64
WINDOW = 128
SP = ("sp_0", "sp_1")
GRP_SP = ("grp", "sp_0", "sp_1")
epsilon = 1e-06


def passed_along(value, axis, steps):
    count = lax.axis_size(axis)
    leading, last = (max(0, -steps), min(count, count - steps))
    return lax.ppermute(value, axis, [(source, source + steps) for source in range(leading, last)])


def split_up(array, dim, size):
    shape = array.shape
    blocks = array.reshape(*shape[:dim], size, shape[dim] // size, *shape[dim + 1 :])
    return jnp.moveaxis(blocks, dim, 0)


def sent_and_summed(array, axis, dim):
    size = lax.axis_size(axis)
    blocks = lax.all_to_all(split_up(array, dim, size), axis, 0, 0, tiled=True)
    return jnp.sum(blocks.astype(jnp.float32), axis=0)


def sent_to_all(array, axis):
    size = lax.axis_size(axis)
    return lax.all_to_all(
        jnp.broadcast_to(array[None], (size, *array.shape)), axis, 0, 0, tiled=True
    )


def in_order(blocks, dim):
    blocks = jnp.moveaxis(blocks, 0, dim)
    shape = blocks.shape
    return blocks.reshape(*shape[:dim], shape[dim] * shape[dim + 1], *shape[dim + 2 :])


def collect(array, axis, dim):
    blocks = sent_to_all(array, axis)
    return in_order(blocks, dim)


def moved_by_axis(blocks, axes, order):
    shape = [lax.axis_size(a) for a in axes]
    blocks = blocks.reshape(*shape, *blocks.shape[1:])
    for k in order:
        blocks = lax.all_to_all(blocks, axes[k], split_axis=k, concat_axis=k, tiled=True)
    return blocks.reshape(-1, *blocks.shape[len(axes) :])


def two_step_exchange(array, groups, order, split_dim, concat_dim):
    size = lax.axis_size(groups[0]) * lax.axis_size(groups[1])
    blocks = split_up(array, split_dim, size)
    return in_order(moved_by_axis(blocks, groups, order), concat_dim)


def sent_together(arrays, axis, dim, along):
    ends, at = ([], 0)
    for a in arrays[:-1]:
        at += a.shape[along]
        ends.append(at)
    both = jnp.concatenate(arrays, axis=along)
    return tuple(jnp.split(lax.all_gather(both, axis, axis=dim, tiled=True), ends, axis=along))


def banded(prev_rows, own_rows, window_len):
    blocks = own_rows.shape[0] // window_len
    joined = jnp.concatenate([prev_rows, own_rows], axis=0)
    shaped = joined.reshape((blocks + 1, window_len) + own_rows.shape[1:])
    return jnp.concatenate([shaped[:-1], shaped[1:]], axis=1)


def shards(
    residual,
    queries,
    keys,
    values,
    segments,
    routes,
    route_weight,
    sinks,
    out_weight,
    norm_gain,
    expert_gate,
    expert_up,
    expert_down,
    shared_gate,
    shared_up,
    shared_down,
):
    rows_here = residual.shape[0]
    model_width = residual.shape[1]
    tp_count = lax.axis_size("tp")
    tp_index = lax.axis_index("tp")
    head_local = queries.shape[1] // HEAD_DIM
    kv_local = keys.shape[1] // HEAD_DIM
    group_size = head_local // kv_local
    window_len = WINDOW
    blocks = rows_here // window_len
    own_marks = (segments % 256 + 1).astype(jnp.bfloat16)
    prev_keys, prev_values, prev_marks = passed_along(
        (
            keys[rows_here - window_len :],
            values[rows_here - window_len :],
            own_marks[rows_here - window_len :],
        ),
        SP,
        1,
    )
    key_band = banded(prev_keys, keys, window_len).reshape(
        blocks, 2 * window_len, kv_local, HEAD_DIM
    )
    value_band = banded(prev_values, values, window_len).reshape(
        blocks, 2 * window_len, kv_local, HEAD_DIM
    )
    mark_band = banded(prev_marks, own_marks, window_len).astype(jnp.float32)
    query_marks = own_marks.reshape(blocks, window_len).astype(jnp.float32)
    query_blocks = queries.reshape(blocks, window_len, kv_local, group_size, HEAD_DIM)
    scores = jnp.einsum(
        "nqhgd,nkhd->nhgqk", query_blocks, key_band, preferred_element_type=jnp.float32
    ) * HEAD_DIM ** (-0.5)
    offsets = jnp.arange(window_len)[:, None] + window_len - jnp.arange(2 * window_len)[None, :]
    allowed = (
        (offsets >= 0) & (offsets < window_len) & (query_marks[:, :, None] == mark_band[:, None, :])
    )
    sink_logits = sinks.reshape(kv_local, group_size)[None, :, :, None]
    masked = jnp.where(allowed[:, None, None], scores, -jnp.inf)
    top_score = jnp.maximum(jnp.max(masked, axis=-1), sink_logits)
    exp_terms = jnp.where(allowed[:, None, None], jnp.exp(scores - top_score[..., None]), 0.0)
    denominator = jnp.sum(exp_terms, axis=-1) + jnp.exp(sink_logits - top_score)
    probabilities = (exp_terms / denominator[..., None]).astype(jnp.bfloat16)
    attended = jnp.einsum(
        "nhgqk,nkhd->nqhgd", probabilities, value_band, preferred_element_type=jnp.float32
    )
    attended = attended.astype(jnp.bfloat16).reshape(rows_here, head_local * HEAD_DIM)
    partial_value = jnp.dot(attended, out_weight, preferred_element_type=jnp.float32)
    col_width = model_width // tp_count
    col_start = tp_index * col_width
    share_sum = sent_and_summed(partial_value.astype(jnp.bfloat16), "tp", 1)
    residual_cols = lax.dynamic_slice_in_dim(residual, col_start, col_width, 1)
    updated_cols = (residual_cols.astype(jnp.float32) + share_sum).astype(jnp.bfloat16)
    cols_f32 = updated_cols.astype(jnp.float32)
    squares = lax.psum(jnp.sum(cols_f32 * cols_f32, axis=-1), "tp")
    inv_rms = lax.rsqrt(squares / model_width + epsilon)
    gain_cols = lax.dynamic_slice_in_dim(norm_gain, col_start, col_width, 0)
    normed_cols = (cols_f32 * inv_rms[:, None] * gain_cols).astype(jnp.bfloat16)
    normed = collect(normed_cols, "tp", 1)
    shared_pre = jnp.dot(normed, shared_gate, preferred_element_type=jnp.float32)
    shared_lin = jnp.dot(normed, shared_up, preferred_element_type=jnp.float32)
    shared_act = (jax.nn.silu(shared_pre) * shared_lin).astype(jnp.bfloat16)
    top_count = routes.shape[1]
    experts = lax.axis_size(SP)
    capacity = 2 * rows_here * top_count // experts
    flat_ids = routes.reshape(-1)
    one_hot = (flat_ids[:, None] == jnp.arange(experts, dtype=jnp.int32)[None, :]).astype(jnp.int32)
    rank_in = jnp.cumsum(one_hot, axis=0) - one_hot
    slot_dest = flat_ids * capacity + jnp.sum(rank_in * one_hot, axis=1)
    token_of = jnp.arange(rows_here * top_count, dtype=jnp.int32) // top_count
    slot_token = jnp.full((experts * capacity,), -1, jnp.int32).at[slot_dest].set(token_of)
    filled = slot_token >= 0
    safe_token = jnp.where(filled, slot_token, 0)
    outgoing = jnp.where(filled[:, None], normed_cols[safe_token], jnp.zeros((), jnp.bfloat16))
    pieces = two_step_exchange(
        outgoing.reshape(experts, capacity, col_width), ("sp_0", "sp_1"), (1, 0), 0, 0
    )
    arrived = lax.all_gather(pieces, "tp", axis=2, tiled=True)
    expert_rows = arrived.reshape(-1, model_width)
    gate_pre = jnp.dot(expert_rows, expert_gate[0], preferred_element_type=jnp.float32)
    up_lin = jnp.dot(expert_rows, expert_up[0], preferred_element_type=jnp.float32)
    expert_act = (jax.nn.silu(gate_pre) * up_lin).astype(jnp.bfloat16)
    gathered_expert, gathered_shared = sent_together((expert_act, shared_act), "tp", 1, 0)
    expert_out = jnp.dot(
        gathered_expert, expert_down[0], preferred_element_type=jnp.float32
    ).astype(jnp.bfloat16)
    returned = lax.all_to_all(
        expert_out.reshape(experts, capacity, col_width),
        SP,
        split_axis=0,
        concat_axis=0,
        tiled=True,
    )
    returned = returned.reshape(experts * capacity, col_width)
    picked = returned[slot_dest].astype(jnp.float32).reshape(rows_here, top_count, col_width)
    routed = jnp.sum(picked * route_weight[:, :, None], axis=1)
    shared_cols = jnp.dot(gathered_shared, shared_down, preferred_element_type=jnp.float32)
    return (updated_cols.astype(jnp.float32) + shared_cols + routed).astype(jnp.bfloat16)


def solution(mesh):
    torus = Mesh(
        mesh.devices.reshape(mesh.shape["grp"], 16, 2, mesh.shape["tp"]),
        ("grp", "sp_0", "sp_1", "tp"),
    )
    in_specs = (
        P(GRP_SP, None),
        P(GRP_SP, "tp"),
        P(GRP_SP, "tp"),
        P(GRP_SP, "tp"),
        P(GRP_SP),
        P(GRP_SP, None),
        P(GRP_SP, None),
        P("tp"),
        P("tp", None),
        P(),
        P(SP, None, "tp"),
        P(SP, None, "tp"),
        P(SP, None, "tp"),
        P(None, "tp"),
        P(None, "tp"),
        P(None, "tp"),
    )
    out_specs = P(GRP_SP, "tp")
    return jax.shard_map(
        shards, mesh=torus, in_specs=in_specs, out_specs=out_specs, check_vma=False
    )
```

profile of v0, /device:TPU:65, one launch (start us, length us, event | category | flops | bytes accessed | tf_op | source)
XLA Modules:
  0.0 356.7 jit_solution(9728244078039882902)
XLA Ops:
  7.3 7.1 %collective-permute-start.1 = (bf16[128]{0:T(256)(128)(2,1)S(1)}, bf16[128]{0:T(256)(128)(2,1)S(1)}, u32[]{:S(2)}, u32[]{:S(2)}) collective-permute-start(bf16[128]{0:T(256)(128)(2,1)S(1)} %slice.57), channel_id=1, source_target_pairs={{0,8},{8,16},{16,24},{24,32},{32,40},{40,48},{48,56},{56,64},{64,7... | collective-permute-start | bytes 776 | tf_op jit(solution)/shard_map/ppermute | solution.py:17
  15.1 1.9 collective-permute-start.2
  17.8 6.1 %collective-permute-start = (bf16[128,64]{0,1:T(8,128)(2,1)S(1)}, bf16[128,64]{0,1:T(8,128)(2,1)S(1)}, u32[]{:S(2)}, u32[]{:S(2)}) collective-permute-start(bf16[128,64]{0,1:T(8,128)(2,1)S(1)} %slice.53), channel_id=1, source_target_pairs={{0,8},{8,16},{16,24},{24,32},{32,40},{40,48},{48,56},{56,64},{64,7... | collective-permute-start | bytes 49160 | tf_op jit(solution)/shard_map/ppermute | solution.py:17
  26.4 24.3 %collective-permute-done.1 = bf16[128]{0:T(256)(128)(2,1)S(1)} collective-permute-done((bf16[128]{0:T(256)(128)(2,1)S(1)}, bf16[128]{0:T(256)(128)(2,1)S(1)}, u32[]{:S(2)}, u32[]{:S(2)}) %collective-permute-start.1) | collective-permute-done | bytes 288 | tf_op jit(solution)/shard_map/ppermute | solution.py:17
  50.8 1.9 collective-permute-done.2
  56.9 1.1 copy.79
  57.9 3.8 %all-to-all-start = ((bf16[8,256,256]{2,1,0:T(8,128)(2,1)}), bf16[8,256,256]{2,1,0:T(8,128)(2,1)S(1)}, u32[]{:S(2)}, u32[]{:S(2)}) async-start(bf16[8,256,256]{2,1,0:T(8,128)(2,1)} %bitcast.106), calls=%async_computation | async-start | bytes 2097152 | tf_op jit(solution)/shard_map/all_to_all | solution.py:28
  62.5 1.2 reduce-window.6
  64.1 2.4 scatter_custom_fusion
  67.4 19.8 %all-to-all-done = bf16[8,256,256]{2,1,0:T(8,128)(2,1)S(1)} async-done(((bf16[8,256,256]{2,1,0:T(8,128)(2,1)}), bf16[8,256,256]{2,1,0:T(8,128)(2,1)S(1)}, u32[]{:S(2)}, u32[]{:S(2)}) %all-to-all-start) | async-done | bytes 1048608 | tf_op jit(solution)/shard_map/all_to_all | solution.py:28
  88.4 11.1 %psum.7 = f32[256]{0:T(256)S(1)} all-reduce(f32[256]{0:T(256)S(1)} %get-tuple-element.5), channel_id=1, replica_groups=mesh['grp'=2,'sp_0'=16,'sp_1'=2,'tp'=8] {'tp'}, use_global_device_ids=true, to_apply=%region_8.9 | all-reduce | flops 256 | bytes 2048 | tf_op jit(solution)/shard_map/psum | solution.py:150
  99.6 3.9 %gather_fusion = bf16[1024,256]{1,0:T(8,128)(2,1)S(1)} fusion(bf16[256,256]{1,0:T(8,128)(2,1)S(1)} %fusion.19, s32[1024]{0:T(1024)S(1)} %fusion.37), kind=kCustom, calls=%fused_computation | custom fusion | bytes 1052672 | tf_op jit(solution)/shard_map/gather | solution.py:169
  103.8 11.5 %all_to_all.25 = bf16[16,2,1,32,256]{4,3,0,2,1:T(8,128)(2,1)S(1)} all-to-all(bf16[16,2,1,32,256]{4,3,0,2,1:T(8,128)(2,1)S(1)} %copy_select_fusion), channel_id=1, replica_groups=mesh['grp'=2,'sp_0'=16,'sp_1'=2,'tp'=8] {'sp_1'}, dimensions={1} | all-to-all | bytes 1048576 | tf_op jit(solution)/shard_map/all_to_all | solution.py:54
  115.3 36.5 %all_to_all.26 = bf16[16,2,1,32,256]{4,3,1,2,0:T(8,128)(2,1)} all-to-all(bf16[16,2,1,32,256]{4,3,1,2,0:T(8,128)(2,1)S(1)} %copy.49), channel_id=1, replica_groups=mesh['grp'=2,'sp_0'=16,'sp_1'=2,'tp'=8] {'sp_0'}, dimensions={0} | all-to-all | bytes 1048576 | tf_op jit(solution)/shard_map/all_to_all | solution.py:54
  152.2 24.5 %all_to_all.27 = bf16[8,256,256]{1,2,0:T(8,128)(2,1)S(1)} all-to-all(bf16[8,256,256]{1,2,0:T(8,128)(2,1)S(1)} %broadcast_in_dim.70), channel_id=1, replica_groups=mesh['grp'=2,'sp_0'=16,'sp_1'=2,'tp'=8] {'tp'}, dimensions={0} | all-to-all | bytes 2097152 | tf_op jit(solution)/shard_map/all_to_all | solution.py:34
  177.6 47.7 %all-gather.3.cloned.1.call-done = bf16[32,32,2048]{2,1,0:T(8,128)(2,1)} async-done(((bf16[32,32,256]{2,1,0:T(8,128)(2,1)}), bf16[32,32,2048]{2,1,0:T(8,128)(2,1)}) %all-gather.3.cloned.1.call-update) | async-done | bytes 4194320 | tf_op jit(solution)/shard_map/all_gather | solution.py:173
  225.3 3.6 %fusion.14 = f32[1024,128]{1,0:T(8,128)S(1)} fusion(bf16[1024,2048]{1,0:T(8,128)(2,1)} %bitcast.108, bf16[1,2048,128]{2,1,0:T(8,128)(2,1)S(1)} %copy-done.2), kind=kOutput, calls=%fused_computation.23 | convolution fusion | flops 536870912 | bytes 5242880 | tf_op jit(solution)/shard_map/dot_general | solution.py:175
  229.0 1.2 fusion.6
  231.0 59.2 %all-gather.5.cloned.1.call-done = bf16[1280,1024]{1,0:T(8,128)(2,1)} async-done(((bf16[1280,128]{1,0:T(8,128)(2,1)}), bf16[1280,1024]{1,0:T(8,128)(2,1)}) %all-gather.5.cloned.1.call-update) | async-done | bytes 2621456 | tf_op jit(solution)/shard_map/all_gather | solution.py:70
  290.2 3.1 fusion.2
  293.3 18.3 %all-to-all-start.4 = ((bf16[32,32,256]{2,1,0:T(8,128)(2,1)}), bf16[32,32,256]{2,1,0:T(8,128)(2,1)S(1)}, u32[]{:S(2)}, u32[]{:S(2)}) async-start(bf16[32,32,256]{2,1,0:T(8,128)(2,1)} %bitcast.25), calls=%async_computation.4 | async-start | bytes 1048576 | tf_op jit(solution)/shard_map/all_to_all | solution.py:182
  311.8 33.1 %all-to-all-done.4 = bf16[32,32,256]{2,1,0:T(8,128)(2,1)S(1)} async-done(((bf16[32,32,256]{2,1,0:T(8,128)(2,1)}), bf16[32,32,256]{2,1,0:T(8,128)(2,1)S(1)}, u32[]{:S(2)}, u32[]{:S(2)}) %all-to-all-start.4) | async-done | bytes 524320 | tf_op jit(solution)/shard_map/all_to_all | solution.py:182
  344.9 1.9 gather_fusion.1
  347.9 2.0 fusion.8
  (80 shorter events, 15.7 us)
Async XLA Ops:
  6.5 49.8 %copy-start = (bf16[128,2048]{1,0:T(8,128)(2,1)S(1)}, bf16[128,2048]{1,0:T(8,128)(2,1)}, u32[]{:S(2)}) copy-start(bf16[128,2048]{1,0:T(8,128)(2,1)} %param.24) | copy-start | bytes 1572868
  7.3 43.4 %collective-permute-start.1 = (bf16[128]{0:T(256)(128)(2,1)S(1)}, bf16[128]{0:T(256)(128)(2,1)S(1)}, u32[]{:S(2)}, u32[]{:S(2)}) collective-permute-start(bf16[128]{0:T(256)(128)(2,1)S(1)} %slice.57), channel_id=1, source_target_pairs={{0,8},{8,16},{16,24},{24,32},{32,40},{40,48},{48,56},{56,64},{64,7... | collective-permute-start | bytes 776 | tf_op jit(solution)/shard_map/ppermute | solution.py:17
  15.1 37.6 %collective-permute-start.2 = (bf16[128,64]{0,1:T(8,128)(2,1)S(1)}, bf16[128,64]{0,1:T(8,128)(2,1)S(1)}, u32[]{:S(2)}, u32[]{:S(2)}) collective-permute-start(bf16[128,64]{0,1:T(8,128)(2,1)S(1)} %slice.60), channel_id=1, source_target_pairs={{0,8},{8,16},{16,24},{24,32},{32,40},{40,48},{48,56},{56,64},{64,7... | collective-permute-start | bytes 49160 | tf_op jit(solution)/shard_map/ppermute | solution.py:17
  17.8 37.6 %collective-permute-start = (bf16[128,64]{0,1:T(8,128)(2,1)S(1)}, bf16[128,64]{0,1:T(8,128)(2,1)S(1)}, u32[]{:S(2)}, u32[]{:S(2)}) collective-permute-start(bf16[128,64]{0,1:T(8,128)(2,1)S(1)} %slice.53), channel_id=1, source_target_pairs={{0,8},{8,16},{16,24},{24,32},{32,40},{40,48},{48,56},{56,64},{64,7... | collective-permute-start | bytes 49160 | tf_op jit(solution)/shard_map/ppermute | solution.py:17
  56.4 5.4 %copy-start.5 = (s32[256,2]{0,1:T(2,128)S(1)}, s32[256,2]{0,1:T(2,128)}, u32[]{:S(2)}) copy-start(s32[256,2]{0,1:T(2,128)} %param.21) | copy-start | bytes 6148
  57.9 29.3 %all-to-all-start = ((bf16[8,256,256]{2,1,0:T(8,128)(2,1)}), bf16[8,256,256]{2,1,0:T(8,128)(2,1)S(1)}, u32[]{:S(2)}, u32[]{:S(2)}) async-start(bf16[8,256,256]{2,1,0:T(8,128)(2,1)} %bitcast.106), calls=%async_computation | async-start | bytes 2097152 | tf_op jit(solution)/shard_map/all_to_all | solution.py:28
  61.7 163.6 %all-gather.3.cloned.1.call-start = ((), (), s32[]{:S(2)}) async-start(), calls=%async_computation.5 | async-start | bytes 4718592 | tf_op jit(solution)/shard_map/all_gather | solution.py:173
  115.3 61.3 %copy-start.4 = (bf16[2048,128]{1,0:T(8,128)(2,1)S(1)}, bf16[2048,128]{1,0:T(8,128)(2,1)}, u32[]{:S(2)}) copy-start(bf16[2048,128]{1,0:T(8,128)(2,1)} %param.29) | copy-start | bytes 1572868
  151.9 25.2 %copy-start.7 = (bf16[2048,128]{1,0:T(8,128)(2,1)S(1)}, bf16[2048,128]{1,0:T(8,128)(2,1)}, u32[]{:S(2)}) copy-start(bf16[2048,128]{1,0:T(8,128)(2,1)} %param.30) | copy-start | bytes 1572868
  151.9 138.3 %all-gather.5.cloned.1.call-start = ((), (), s32[]{:S(2)}) async-start(), calls=%async_computation.6 | async-start | bytes 2949120 | tf_op jit(solution)/shard_map/all_gather | solution.py:70
  152.1 73.2 %copy-start.2 = (bf16[1,2048,128]{2,1,0:T(8,128)(2,1)S(1)}, bf16[1,2048,128]{2,1,0:T(8,128)(2,1)}, u32[]{:S(2)}) copy-start(bf16[1,2048,128]{2,1,0:T(8,128)(2,1)} %param.26) | copy-start | bytes 1572868
  225.3 3.6 %copy-start.1 = (bf16[32,32,2048]{2,1,0:T(8,128)(2,1)S(1)}, bf16[32,32,2048]{2,1,0:T(8,128)(2,1)}, u32[]{:S(2)}) copy-start(bf16[32,32,2048]{2,1,0:T(8,128)(2,1)} %all-gather.3.cloned.1.call-done) | copy-start | bytes 12582916
  225.3 3.6 %copy-start.8 = (bf16[1,2048,128]{2,1,0:T(8,128)(2,1)S(1)}, bf16[1,2048,128]{2,1,0:T(8,128)(2,1)}, u32[]{:S(2)}) copy-start(bf16[1,2048,128]{2,1,0:T(8,128)(2,1)} %param.27) | copy-start | bytes 1572868
  229.0 61.2 %copy-start.9 = (bf16[1,1024,256]{2,1,0:T(8,128)(2,1)S(1)}, bf16[1,1024,256]{2,1,0:T(8,128)(2,1)}, u32[]{:S(2)}) copy-start(bf16[1,1024,256]{2,1,0:T(8,128)(2,1)} %param.28) | copy-start | bytes 1572868
  231.0 80.6 %copy-start.6 = (f32[256,2]{0,1:T(2,128)S(1)}, f32[256,2]{0,1:T(2,128)}, u32[]{:S(2)}) copy-start(f32[256,2]{0,1:T(2,128)} %param.22) | copy-start | bytes 6148
  293.3 54.6 %copy-start.3 = (bf16[1024,256]{1,0:T(8,128)(2,1)S(1)}, bf16[1024,256]{1,0:T(8,128)(2,1)}, u32[]{:S(2)}) copy-start(bf16[1024,256]{1,0:T(8,128)(2,1)} %param.31) | copy-start | bytes 1572868
  293.3 51.6 %all-to-all-start.4 = ((bf16[32,32,256]{2,1,0:T(8,128)(2,1)}), bf16[32,32,256]{2,1,0:T(8,128)(2,1)S(1)}, u32[]{:S(2)}, u32[]{:S(2)}) async-start(bf16[32,32,256]{2,1,0:T(8,128)(2,1)} %bitcast.25), calls=%async_computation.4 | async-start | bytes 1048576 | tf_op jit(solution)/shard_map/all_to_all | solution.py:182
Sparse Core Ops, SparseCore 0:
  152.0 73.2 all-gather.2
  231.1 59.0 all-gather.4
where the time goes:
time: 358 us; the launch traced here: 357 us
  waiting for transfers between devices  186 us (52%)
  blocking collectives  83.5 us (23%)
  starting transfers between devices  37.3 us (10%)
  local copies, waits for them, and re-layouts  15.8 us (4%)
  between operations  13.8 us (4%)
  matrix products  11.9 us (3%)
  other arithmetic  8.26 us (2%)
    all_gather x1, waiting for transfers between devices, sent_together(): lax.all_gather(both, axis, axis=dim, tiled=True)  59.2 us
    all_to_all x2, blocking collectives, moved_by_axis(): lax.all_to_all(blocks, axes[k], split_axis=k, concat_axis=k, tiled=True)  48 us
    all_gather x1, waiting for transfers between devices, shards(): arrived = lax.all_gather(pieces, 'tp', axis=2, tiled=True)  47.7 us
    all_to_all x1, waiting for transfers between devices, shards(): lax.all_to_all(expert_out.reshape(experts, capacity, col_width), SP, spli...  33.1 us
    ppermute x3, waiting for transfers between devices, passed_along(): lax.ppermute(value, axis, [(source, source + steps) for source in range(l...  26.1 us
    all_to_all x1, blocking collectives, sent_to_all(): lax.all_to_all(jnp.broadcast_to(array[None], (size, *array.shape)), axis,...  24.5 us
    all_to_all x1, waiting for transfers between devices, sent_and_summed(): blocks = lax.all_to_all(split_up(array, dim, size), axis, 0, 0, tiled=True)  19.8 us
    all_to_all x1, starting transfers between devices, shards(): lax.all_to_all(expert_out.reshape(experts, capacity, col_width), SP, spli...  18.3 us
  transfers between devices with their start and end apart: 7, of which 6 were waited for; matrix products, arithmetic and copies ran while one was open for 4% of the time, Pallas kernels for 0%

commit v1 on v0

--- a/solution.py
+++ b/solution.py
@@ -170,7 +170,9 @@
     pieces = two_step_exchange(
         outgoing.reshape(experts, capacity, col_width), ("sp_0", "sp_1"), (1, 0), 0, 0
     )
-    arrived = lax.all_gather(pieces, "tp", axis=2, tiled=True)
+    arrived = jnp.concatenate(
+        lax.all_to_all(jnp.stack([pieces] * lax.axis_size("tp")), "tp", 0, 0), axis=2
+    )
     expert_rows = arrived.reshape(-1, model_width)
     gate_pre = jnp.dot(expert_rows, expert_gate[0], preferred_element_type=jnp.float32)
     up_lin = jnp.dot(expert_rows, expert_up[0], preferred_element_type=jnp.float32)

time: 358 us -> 417 us (1.16)
  waiting for transfers between devices: 186 us -> 252 us
  blocking collectives: 83.5 us -> 58.5 us
  local copies, waits for them, and re-layouts: 15.8 us -> 27.3 us
  starting transfers between devices: 37.3 us -> 45.9 us
    all_to_all x0 -> x2, waiting for transfers between devices: none -> 114 us  [the longest x1 86.8 us: shards(): lax.all_to_all(jnp.stack([pieces] * lax.axis_size('tp')), 'tp', 0, 0)]
    all_gather x1 -> x0, waiting for transfers between devices: 47.7 us -> none  [shards(): arrived = lax.all_gather(pieces, 'tp', axis=2, tiled=True)]
    all_to_all x1 -> x0, blocking collectives: 24.5 us -> none  [sent_to_all(): lax.all_to_all(jnp.broadcast_to(array[None], (size, *array.shape)), axis,...]
    all_to_all x0 -> x2, starting transfers between devices: none -> 8.62 us  [the longest x1 4.86 us: shards(): lax.all_to_all(jnp.stack([pieces] * lax.axis_size('tp')), 'tp', 0, 0)]
    reshape x0 -> x1, local copies, waits for them, and re-layouts: none -> 6.47 us  [shards(): jnp.concatenate(lax.all_to_all(jnp.stack([pieces] * lax.axis_size('tp')),...]
  transfers between devices with their start and end apart: 7 -> 8, of which waited for: 6 -> 7; matrix products, arithmetic and copies ran while one was open for 4% -> 3% of each run, Pallas kernels for 0% -> 0%
where the time goes in v1:
time: 417 us; the launch traced here: 416 us
  waiting for transfers between devices  252 us (60%)
  blocking collectives  58.5 us (14%)
  starting transfers between devices  45.9 us (11%)
  local copies, waits for them, and re-layouts  27.3 us (7%)
  between operations  13.8 us (3%)
  matrix products  9.56 us (2%)
  other arithmetic  8.26 us (2%)
    all_to_all x1, waiting for transfers between devices, shards(): lax.all_to_all(jnp.stack([pieces] * lax.axis_size('tp')), 'tp', 0, 0)  86.8 us
    all_gather x1, waiting for transfers between devices, sent_together(): lax.all_gather(both, axis, axis=dim, tiled=True)  59.6 us
    all_to_all x2, blocking collectives, moved_by_axis(): lax.all_to_all(blocks, axes[k], split_axis=k, concat_axis=k, tiled=True)  47.4 us
    all_to_all x1, waiting for transfers between devices, shards(): lax.all_to_all(expert_out.reshape(experts, capacity, col_width), SP, spli...  33.1 us
    all_to_all x1, waiting for transfers between devices, sent_to_all(): lax.all_to_all(jnp.broadcast_to(array[None], (size, *array.shape)), axis,...  26.8 us
    ppermute x3, waiting for transfers between devices, passed_along(): lax.ppermute(value, axis, [(source, source + steps) for source in range(l...  26.1 us
    all_to_all x1, waiting for transfers between devices, sent_and_summed(): blocks = lax.all_to_all(split_up(array, dim, size), axis, 0, 0, tiled=True)  19.9 us
    all_to_all x1, starting transfers between devices, shards(): lax.all_to_all(expert_out.reshape(experts, capacity, col_width), SP, spli...  18.2 us
  transfers between devices with their start and end apart: 8, of which 7 were waited for; matrix products, arithmetic and copies ran while one was open for 3% of the time, Pallas kernels for 0%

profile of v1, /device:TPU:65, one launch (start us, length us, event | category | flops | bytes accessed | tf_op | source)
XLA Modules:
  0.0 415.7 jit_solution(1078981677317244205)
XLA Ops:
  7.3 7.1 %collective-permute-start.1 = (bf16[128]{0:T(256)(128)(2,1)S(1)}, bf16[128]{0:T(256)(128)(2,1)S(1)}, u32[]{:S(2)}, u32[]{:S(2)}) collective-permute-start(bf16[128]{0:T(256)(128)(2,1)S(1)} %slice.57), channel_id=1, source_target_pairs={{0,8},{8,16},{16,24},{24,32},{32,40},{40,48},{48,56},{56,64},{64,7... | collective-permute-start | bytes 776 | tf_op jit(solution)/shard_map/ppermute | solution.py:17
  15.1 1.9 collective-permute-start.2
  17.8 6.1 %collective-permute-start = (bf16[128,64]{0,1:T(8,128)(2,1)S(1)}, bf16[128,64]{0,1:T(8,128)(2,1)S(1)}, u32[]{:S(2)}, u32[]{:S(2)}) collective-permute-start(bf16[128,64]{0,1:T(8,128)(2,1)S(1)} %slice.53), channel_id=1, source_target_pairs={{0,8},{8,16},{16,24},{24,32},{32,40},{40,48},{48,56},{56,64},{64,7... | collective-permute-start | bytes 49160 | tf_op jit(solution)/shard_map/ppermute | solution.py:17
  26.4 24.3 %collective-permute-done.1 = bf16[128]{0:T(256)(128)(2,1)S(1)} collective-permute-done((bf16[128]{0:T(256)(128)(2,1)S(1)}, bf16[128]{0:T(256)(128)(2,1)S(1)}, u32[]{:S(2)}, u32[]{:S(2)}) %collective-permute-start.1) | collective-permute-done | bytes 288 | tf_op jit(solution)/shard_map/ppermute | solution.py:17
  50.8 1.9 collective-permute-done.2
  57.9 3.8 all-to-all-start
  64.0 2.4 scatter_custom_fusion
  67.3 19.9 %all-to-all-done = bf16[8,256,256]{2,1,0:T(8,128)(2,1)S(1)} async-done(((bf16[8,256,256]{2,1,0:T(8,128)(2,1)}), bf16[8,256,256]{2,1,0:T(8,128)(2,1)S(1)}, u32[]{:S(2)}, u32[]{:S(2)}) %all-to-all-start) | async-done | bytes 1048608 | tf_op jit(solution)/shard_map/all_to_all | solution.py:28
  88.4 11.1 %psum.7 = f32[256]{0:T(256)S(1)} all-reduce(f32[256]{0:T(256)S(1)} %get-tuple-element.5), channel_id=1, replica_groups=mesh['grp'=2,'sp_0'=16,'sp_1'=2,'tp'=8] {'tp'}, use_global_device_ids=true, to_apply=%region_8.9 | all-reduce | flops 256 | bytes 2048 | tf_op jit(solution)/shard_map/psum | solution.py:150
  99.7 3.9 gather_fusion
  103.8 11.5 %all_to_all.30 = bf16[16,2,1,32,256]{4,3,0,2,1:T(8,128)(2,1)S(1)} all-to-all(bf16[16,2,1,32,256]{4,3,0,2,1:T(8,128)(2,1)S(1)} %copy_select_fusion), channel_id=1, replica_groups=mesh['grp'=2,'sp_0'=16,'sp_1'=2,'tp'=8] {'sp_1'}, dimensions={1} | all-to-all | bytes 1048576 | tf_op jit(solution)/shard_map/all_to_all | solution.py:54
  116.4 3.8 all-to-all-start.4
  120.2 26.8 %all-to-all-done.4 = bf16[8,256,256]{1,2,0:T(8,128)(2,1)S(1)} async-done(((bf16[8,256,256]{1,2,0:T(8,128)(2,1)}), bf16[8,256,256]{1,2,0:T(8,128)(2,1)S(1)}, u32[]{:S(2)}, u32[]{:S(2)}) %all-to-all-start.4) | async-done | bytes 1048608 | tf_op jit(solution)/shard_map/all_to_all | solution.py:34
  147.0 35.9 %all_to_all.31 = bf16[16,2,1,32,256]{4,3,1,2,0:T(8,128)(2,1)S(1)} all-to-all(bf16[16,2,1,32,256]{4,3,1,2,0:T(8,128)(2,1)S(1)} %copy.49), channel_id=1, replica_groups=mesh['grp'=2,'sp_0'=16,'sp_1'=2,'tp'=8] {'sp_0'}, dimensions={0} | all-to-all | bytes 1048576 | tf_op jit(solution)/shard_map/all_to_all | solution.py:54
  182.9 2.5 stack.3
  185.4 4.9 %all-to-all-start.3 = ((bf16[8,32,32,256]{3,2,1,0:T(8,128)(2,1)}), bf16[8,32,32,256]{3,2,1,0:T(8,128)(2,1)}, u32[]{:S(2)}, u32[]{:S(2)}) async-start(bf16[8,32,32,256]{3,2,1,0:T(8,128)(2,1)} %stack.3), calls=%async_computation.3 | async-start | bytes 8388608 | tf_op jit(solution)/shard_map/all_to_all | solution.py:174
  191.5 86.8 %all-to-all-done.3 = bf16[8,32,32,256]{3,2,1,0:T(8,128)(2,1)} async-done(((bf16[8,32,32,256]{3,2,1,0:T(8,128)(2,1)}), bf16[8,32,32,256]{3,2,1,0:T(8,128)(2,1)}, u32[]{:S(2)}, u32[]{:S(2)}) %all-to-all-start.3) | async-done | bytes 4194336 | tf_op jit(solution)/shard_map/all_to_all | solution.py:174
  278.3 6.5 %copy.50 = bf16[32,32,8,256]{3,2,1,0:T(8,128)(2,1)S(1)} copy(bf16[32,32,8,256]{3,1,0,2:T(8,128)(2,1)} %bitcast.18) | data formatting | bytes 8388608 | tf_op jit(solution)/shard_map/reshape | solution.py:173
  289.6 59.6 %all-gather.2.cloned.1.call-done = bf16[1280,1024]{1,0:T(8,128)(2,1)} async-done(((bf16[1280,128]{1,0:T(8,128)(2,1)}), bf16[1280,1024]{1,0:T(8,128)(2,1)}) %all-gather.2.cloned.1.call-update) | async-done | bytes 2621456 | tf_op jit(solution)/shard_map/all_gather | solution.py:70
  349.2 3.1 fusion.2
  352.4 18.2 %all-to-all-start.5 = ((bf16[32,32,256]{2,1,0:T(8,128)(2,1)}), bf16[32,32,256]{2,1,0:T(8,128)(2,1)S(1)}, u32[]{:S(2)}, u32[]{:S(2)}) async-start(bf16[32,32,256]{2,1,0:T(8,128)(2,1)} %bitcast.25), calls=%async_computation.5 | async-start | bytes 1048576 | tf_op jit(solution)/shard_map/all_to_all | solution.py:184
  370.7 33.1 %all-to-all-done.5 = bf16[32,32,256]{2,1,0:T(8,128)(2,1)S(1)} async-done(((bf16[32,32,256]{2,1,0:T(8,128)(2,1)}), bf16[32,32,256]{2,1,0:T(8,128)(2,1)S(1)}, u32[]{:S(2)}, u32[]{:S(2)}) %all-to-all-start.5) | async-done | bytes 524320 | tf_op jit(solution)/shard_map/all_to_all | solution.py:184
  403.9 1.9 gather_fusion.1
  406.8 2.0 fusion.8
  (81 shorter events, 23.0 us)
Async XLA Ops:
  6.5 49.8 %copy-start = (bf16[128,2048]{1,0:T(8,128)(2,1)S(1)}, bf16[128,2048]{1,0:T(8,128)(2,1)}, u32[]{:S(2)}) copy-start(bf16[128,2048]{1,0:T(8,128)(2,1)} %param.24) | copy-start | bytes 1572868
  7.3 43.4 %collective-permute-start.1 = (bf16[128]{0:T(256)(128)(2,1)S(1)}, bf16[128]{0:T(256)(128)(2,1)S(1)}, u32[]{:S(2)}, u32[]{:S(2)}) collective-permute-start(bf16[128]{0:T(256)(128)(2,1)S(1)} %slice.57), channel_id=1, source_target_pairs={{0,8},{8,16},{16,24},{24,32},{32,40},{40,48},{48,56},{56,64},{64,7... | collective-permute-start | bytes 776 | tf_op jit(solution)/shard_map/ppermute | solution.py:17
  15.1 37.6 %collective-permute-start.2 = (bf16[128,64]{0,1:T(8,128)(2,1)S(1)}, bf16[128,64]{0,1:T(8,128)(2,1)S(1)}, u32[]{:S(2)}, u32[]{:S(2)}) collective-permute-start(bf16[128,64]{0,1:T(8,128)(2,1)S(1)} %slice.60), channel_id=1, source_target_pairs={{0,8},{8,16},{16,24},{24,32},{32,40},{40,48},{48,56},{56,64},{64,7... | collective-permute-start | bytes 49160 | tf_op jit(solution)/shard_map/ppermute | solution.py:17
  17.8 37.6 %collective-permute-start = (bf16[128,64]{0,1:T(8,128)(2,1)S(1)}, bf16[128,64]{0,1:T(8,128)(2,1)S(1)}, u32[]{:S(2)}, u32[]{:S(2)}) collective-permute-start(bf16[128,64]{0,1:T(8,128)(2,1)S(1)} %slice.53), channel_id=1, source_target_pairs={{0,8},{8,16},{16,24},{24,32},{32,40},{40,48},{48,56},{56,64},{64,7... | collective-permute-start | bytes 49160 | tf_op jit(solution)/shard_map/ppermute | solution.py:17
  56.1 5.6 %copy-start.4 = (s32[256,2]{0,1:T(2,128)S(1)}, s32[256,2]{0,1:T(2,128)}, u32[]{:S(2)}) copy-start(s32[256,2]{0,1:T(2,128)} %param.21) | copy-start | bytes 6148
  57.9 29.3 %all-to-all-start = ((bf16[8,256,256]{2,1,0:T(8,128)(2,1)}), bf16[8,256,256]{2,1,0:T(8,128)(2,1)S(1)}, u32[]{:S(2)}, u32[]{:S(2)}) async-start(bf16[8,256,256]{2,1,0:T(8,128)(2,1)} %bitcast.109), calls=%async_computation | async-start | bytes 2097152 | tf_op jit(solution)/shard_map/all_to_all | solution.py:28
  116.4 30.6 %all-to-all-start.4 = ((bf16[8,256,256]{1,2,0:T(8,128)(2,1)}), bf16[8,256,256]{1,2,0:T(8,128)(2,1)S(1)}, u32[]{:S(2)}, u32[]{:S(2)}) async-start(bf16[8,256,256]{1,2,0:T(8,128)(2,1)} %broadcast_in_dim.70), calls=%async_computation.4 | async-start | bytes 2097152 | tf_op jit(solution)/shard_map/all_to_all | solution.py:34
  185.4 5.1 %copy-start.3 = (bf16[2048,128]{1,0:T(8,128)(2,1)S(1)}, bf16[2048,128]{1,0:T(8,128)(2,1)}, u32[]{:S(2)}) copy-start(bf16[2048,128]{1,0:T(8,128)(2,1)} %param.29) | copy-start | bytes 1572868
  185.4 5.6 %copy-start.6 = (bf16[2048,128]{1,0:T(8,128)(2,1)S(1)}, bf16[2048,128]{1,0:T(8,128)(2,1)}, u32[]{:S(2)}) copy-start(bf16[2048,128]{1,0:T(8,128)(2,1)} %param.30) | copy-start | bytes 1572868
  185.4 92.9 %all-to-all-start.3 = ((bf16[8,32,32,256]{3,2,1,0:T(8,128)(2,1)}), bf16[8,32,32,256]{3,2,1,0:T(8,128)(2,1)}, u32[]{:S(2)}, u32[]{:S(2)}) async-start(bf16[8,32,32,256]{3,2,1,0:T(8,128)(2,1)} %stack.3), calls=%async_computation.3 | async-start | bytes 8388608 | tf_op jit(solution)/shard_map/all_to_all | solution.py:174
  190.3 159.0 %all-gather.2.cloned.1.call-start = ((), (), s32[]{:S(2)}) async-start(), calls=%async_computation.6 | async-start | bytes 2949120 | tf_op jit(solution)/shard_map/all_gather | solution.py:70
  284.7 1.5 copy-start.1
  286.2 1.3 copy-start.7
  287.5 61.7 %copy-start.8 = (bf16[1,1024,256]{2,1,0:T(8,128)(2,1)S(1)}, bf16[1,1024,256]{2,1,0:T(8,128)(2,1)}, u32[]{:S(2)}) copy-start(bf16[1,1024,256]{2,1,0:T(8,128)(2,1)} %param.28) | copy-start | bytes 1572868
  288.8 81.8 %copy-start.5 = (f32[256,2]{0,1:T(2,128)S(1)}, f32[256,2]{0,1:T(2,128)}, u32[]{:S(2)}) copy-start(f32[256,2]{0,1:T(2,128)} %param.22) | copy-start | bytes 6148
  289.6 117.2 %copy-start.2 = (bf16[1024,256]{1,0:T(8,128)(2,1)S(1)}, bf16[1024,256]{1,0:T(8,128)(2,1)}, u32[]{:S(2)}) copy-start(bf16[1024,256]{1,0:T(8,128)(2,1)} %param.31) | copy-start | bytes 1572868
  352.4 51.5 %all-to-all-start.5 = ((bf16[32,32,256]{2,1,0:T(8,128)(2,1)}), bf16[32,32,256]{2,1,0:T(8,128)(2,1)S(1)}, u32[]{:S(2)}, u32[]{:S(2)}) async-start(bf16[32,32,256]{2,1,0:T(8,128)(2,1)} %bitcast.25), calls=%async_computation.5 | async-start | bytes 1048576 | tf_op jit(solution)/shard_map/all_to_all | solution.py:184
Sparse Core Ops, SparseCore 0:
  289.7 59.4 all-gather.1
